TPU v7x, 32 devices: a whole 2x2x4 slice. The times are simulated.
32 devices in a mesh: tp: 8 (over z, core), dp: 4 (over y, x).
Axes of the slice: x: 2, y: 2, z: 4, core: 2. Of those that a mesh axis runs over, the one named last changes fastest.
Arguments:
- tokens: bfloat16 [32, 4096], P('tp', 'dp'), may hold values from -6 to 6
- norm_gain: bfloat16 [2, 4096], P(None, 'dp'), may hold values from 0.099609375 to 1.8984375
- w_query: bfloat16 [2, 4096, 1024], P(None, 'dp', 'tp'), may hold values from -0.09375 to 0.09375
- w_key: bfloat16 [2, 4096, 1024], P(None, 'dp', 'tp'), may hold values from -0.09375 to 0.09375
- w_value: bfloat16 [2, 4096, 1024], P(None, 'dp', 'tp'), may hold values from -0.09375 to 0.09375
- w_outgate: bfloat16 [2, 4096, 1024], P(None, 'dp', 'tp'), may hold values from -0.09375 to 0.09375
- w_gates: bfloat16 [2, 4096, 16], P(None, 'dp'), may hold values from -0.09375 to 0.09375
- gate_bias: float32 [2, 2, 8], P(None, None, 'tp'), may hold values from -1 to 5
- w_out: bfloat16 [2, 1024, 4096], P(None, 'tp', 'dp'), may hold values from -0.1875 to 0.1875
- memory: float32 [2, 32, 8, 128, 128], P(None, 'dp', 'tp'), may hold values from -6 to 6
- normalizer: float32 [2, 32, 8, 128], P(None, 'dp', 'tp'), may hold values from -3 to 3
- stabilizer: float32 [2, 32, 8], P(None, 'dp', 'tp'), may hold values from -8 to 300, as said below
Outputs:
- mixed: bfloat16 [32, 4096], P('tp', 'dp')
- new_memory: float32 [2, 32, 8, 128, 128], P(None, 'dp', 'tp')
- new_normalizer: float32 [2, 32, 8, 128], P(None, 'dp', 'tp')
- new_stabilizer: float32 [2, 32, 8], P(None, 'dp', 'tp')
Inputs may be any that keep to these rules, and one draw needn't show every extreme that they name: `stabilizer`: lies between -8 and 8, except that some entries may be as large as 300.
All inputs are finite; a program needn't handle non-finite values.
Results may differ from a plain program's by a relative error of at most 0.04.
Values may be sent and summed in bfloat16 or wider, within the bound.
A program may use at most 64 MiB of HBM per device.

v0:
```python
import jax
import jax.numpy as jnp
from jax import lax
from jax.sharding import PartitionSpec as P

D = 4096
HEAD_SIZE = 128
epsilon = 1e-06


def cell_update(query, key_rows, value_rows, input_pre, forget_pre, memory, normalizer, stabilizer):
    batch_size = query.shape[0]
    head_count = input_pre.shape[1]
    query_float = query.astype(jnp.float32).reshape(batch_size, head_count, -1)
    key_float = key_rows.astype(jnp.float32).reshape(
        batch_size, head_count, -1
    ) * query_float.shape[2] ** (-0.5)
    value_float = value_rows.astype(jnp.float32).reshape(batch_size, head_count, -1)
    carried = jax.nn.log_sigmoid(forget_pre) + stabilizer
    new_max = jnp.maximum(carried, input_pre)
    keep_factor = jnp.exp(carried - new_max)
    write_factor = jnp.exp(input_pre - new_max)
    new_memory = (
        keep_factor[:, :, None, None] * memory
        + write_factor[:, :, None, None] * value_float[:, :, :, None] * key_float[:, :, None, :]
    )
    new_normalizer = keep_factor[:, :, None] * normalizer + write_factor[:, :, None] * key_float
    numerator = jnp.sum(new_memory * query_float[:, :, None, :], axis=3)
    denominator = jnp.sum(new_normalizer * query_float, axis=2)
    floor_value = jnp.maximum(jnp.abs(denominator), jnp.exp(-new_max))
    readout = numerator / jnp.maximum(floor_value, 1.0)[:, :, None]
    return (readout.reshape(batch_size, -1), new_memory, new_normalizer, new_max)


def finish_split(partial_out, wide_rows):
    summed = lax.psum_scatter(partial_out, "tp", scatter_dimension=0, tiled=True)
    own_rows = lax.dynamic_slice_in_dim(
        wide_rows, lax.axis_index("tp") * summed.shape[0], summed.shape[0], 0
    )
    return (own_rows + summed).astype(jnp.bfloat16)


def body(
    tokens,
    norm_gain,
    w_query,
    w_key,
    w_value,
    w_outgate,
    w_gates,
    gate_bias,
    w_out,
    memory,
    normalizer,
    stabilizer,
):
    heads_here = w_query.shape[2] // HEAD_SIZE
    seq_here = memory.shape[1]
    all_heads = w_gates.shape[2] // 2
    head_first = lax.axis_index("tp") * heads_here
    seq_first = lax.axis_index("dp") * seq_here
    current = tokens
    gathered = None
    memories = []
    normalizers = []
    maxima = []
    for layer_index in range(2):
        if gathered is None:
            gathered = lax.all_gather(current, "tp", axis=0, tiled=True)
        wide_rows = gathered.astype(jnp.float32)
        square_part = jnp.sum(wide_rows * wide_rows, axis=1)
        scaled = (wide_rows * norm_gain[layer_index].astype(jnp.float32)[None, :]).astype(
            jnp.bfloat16
        )
        gate_weight = w_gates[layer_index]
        own_gates = jnp.concatenate(
            [
                lax.dynamic_slice_in_dim(gate_weight, head_first, heads_here, 1),
                lax.dynamic_slice_in_dim(gate_weight, all_heads + head_first, heads_here, 1),
            ],
            axis=1,
        )
        term_query = jnp.dot(scaled, w_query[layer_index], preferred_element_type=jnp.float32)
        term_key = jnp.dot(scaled, w_key[layer_index], preferred_element_type=jnp.float32)
        term_value = jnp.dot(scaled, w_value[layer_index], preferred_element_type=jnp.float32)
        term_outgate = jnp.dot(scaled, w_outgate[layer_index], preferred_element_type=jnp.float32)
        term_gates = jnp.dot(scaled, own_gates, preferred_element_type=jnp.float32)
        square_all = lax.psum(square_part, "dp")
        square_own = lax.dynamic_slice_in_dim(square_all, seq_first, seq_here, 0)
        sum_query, sum_key, sum_value, sum_outgate, sum_gates = (
            lax.psum_scatter(term_query, "dp", scatter_dimension=0, tiled=True),
            lax.psum_scatter(term_key, "dp", scatter_dimension=0, tiled=True),
            lax.psum_scatter(term_value, "dp", scatter_dimension=0, tiled=True),
            lax.psum_scatter(term_outgate, "dp", scatter_dimension=0, tiled=True),
            lax.psum_scatter(term_gates, "dp", scatter_dimension=0, tiled=True),
        )
        inv_scale = lax.rsqrt(square_own / D + epsilon)[:, None]
        query = (sum_query * inv_scale).astype(jnp.bfloat16)
        key_rows = (sum_key * inv_scale).astype(jnp.bfloat16)
        value_rows = (sum_value * inv_scale).astype(jnp.bfloat16)
        outgate = (sum_outgate * inv_scale).astype(jnp.bfloat16)
        gate_pre = sum_gates * inv_scale
        bias_here = gate_bias[layer_index]
        input_pre = gate_pre[:, :heads_here] + bias_here[0][None, :]
        forget_pre = gate_pre[:, heads_here:] + bias_here[1][None, :]
        readout, new_memory, new_normalizer, new_max = cell_update(
            query,
            key_rows,
            value_rows,
            input_pre,
            forget_pre,
            memory[layer_index],
            normalizer[layer_index],
            stabilizer[layer_index],
        )
        gated = (jax.nn.sigmoid(outgate.astype(jnp.float32)) * readout).astype(jnp.bfloat16)
        out_weight = w_out[layer_index]
        partial_out = jnp.dot(
            lax.all_gather(gated, "dp", axis=0, tiled=True),
            out_weight,
            preferred_element_type=jnp.float32,
        )
        if layer_index == 0:
            summed = lax.psum(partial_out, "tp")
            gathered = (wide_rows + summed).astype(jnp.bfloat16)
        else:
            current = finish_split(partial_out, wide_rows)
        memories.append(new_memory)
        normalizers.append(new_normalizer)
        maxima.append(new_max)
    return (current, jnp.stack(memories), jnp.stack(normalizers), jnp.stack(maxima))


def solution(mesh):
    placed = (
        P("tp", "dp"),
        P(None, "dp"),
        P(None, "dp", "tp"),
        P(None, "dp", "tp"),
        P(None, "dp", "tp"),
        P(None, "dp", "tp"),
        P(None, "dp", None),
        P(None, None, "tp"),
        P(None, "tp", "dp"),
        P(None, "dp", "tp", None, None),
        P(None, "dp", "tp", None),
        P(None, "dp", "tp"),
    )
    return jax.shard_map(
        body,
        mesh=mesh,
        in_specs=placed,
        out_specs=(
            P("tp", "dp"),
            P(None, "dp", "tp", None, None),
            P(None, "dp", "tp", None),
            P(None, "dp", "tp"),
        ),
        check_vma=False,
    )
```

profile of v0, /device:TPU:0, one launch (start us, length us, event | category | flops | bytes accessed | tf_op | source)
XLA Modules:
  0.0 269.4 jit_solution(6725401215718095154)
XLA Ops:
  7.2 0.8 slice_convert_fusion
  8.0 15.9 %all-gather = bf16[8,4,1024]{2,1,0:T(4,128)(2,1)S(1)} all-gather(bf16[1,4,1024]{2,1,0:T(4,128)(2,1)} %bitcast.146), channel_id=1, replica_groups=mesh['tp'=8,'dp'=4] {'tp'}, dimensions={0}, use_global_device_ids=true | all-gather | bytes 73728 | tf_op jit(solution)/shard_map/all_gather | solution.py:69
  24.6 1.7 fusion.18
  26.3 0.8 fusion.20
  27.1 0.8 fusion.22
  27.9 1.8 fusion.24
  29.7 0.7 fusion.42
  32.4 40.8 %all-reduce.24.cloned.1.call-done = (f32[32,128]{1,0:T(8,128)}, f32[32]{0:T(128)}, f32[32,128]{1,0:T(8,128)}, f32[32,128]{1,0:T(8,128)}, f32[32,2]{0,1:T(2,128)}, /*index=5*/f32[32,128]{1,0:T(8,128)}) async-done(((f32[32,128]{1,0:T(8,128)}, f32[32]{0:T(128)}, f32[32,128]{1,0:T(8,128)}, f32[32,128]{1,0:T(8,128)}, f32[32,2]{0,1:T(2,128)}, /*index=5*/f32[32,128]{1,0:T(8,128)}), (f32[32,128]{1,0:T(8,128)}, ...) | async-done | bytes 65936
  73.2 0.7 add_rsqrt_fusion.1
  74.0 0.7 fusion.62
  74.7 1.4 broadcast_multiply_fusion.1
  76.1 0.8 fusion.59
  76.8 0.9 multiply_reduce_fusion.3
  78.1 0.8 multiply_convert_fusion.3
  78.9 8.9 %all_gather.10 = bf16[32,128]{1,0:T(8,128)(2,1)S(1)} all-gather(bf16[8,128]{1,0:T(8,128)(2,1)S(1)} %multiply_convert_fusion.3), channel_id=1, replica_groups=mesh['tp'=8,'dp'=4] {'dp'}, dimensions={0}, use_global_device_ids=true | all-gather | bytes 10240 | tf_op jit(solution)/shard_map/all_gather | solution.py:119
  87.8 0.8 fusion.16
  88.7 55.4 %all-reduce.18.cloned.1.call-done = f32[32,1024]{1,0:T(8,128)} async-done(((f32[32,1024]{1,0:T(8,128)}), f32[32,1024]{1,0:T(8,128)}) %all-reduce.18.cloned.1.call-update) | async-done | bytes 131088 | tf_op jit(solution)/shard_map/psum | solution.py:124
  144.1 1.5 multiply_reduce_fusion
  145.7 0.8 fusion.8
  146.5 0.8 fusion.10
  147.2 0.8 fusion.12
  148.0 0.8 fusion.14
  151.4 38.9 %all-reduce.22.cloned.1.call-done = (f32[32,128]{1,0:T(8,128)}, f32[32]{0:T(128)}, f32[32,128]{1,0:T(8,128)}, f32[32,128]{1,0:T(8,128)}, f32[32,2]{0,1:T(2,128)}, /*index=5*/f32[32,128]{1,0:T(8,128)}) async-done(((f32[32,128]{1,0:T(8,128)}, f32[32]{0:T(128)}, f32[32,128]{1,0:T(8,128)}, f32[32,128]{1,0:T(8,128)}, f32[32,2]{0,1:T(2,128)}, /*index=5*/f32[32,128]{1,0:T(8,128)}), (f32[32,128]{1,0:T(8,128)}, ...) | async-done | bytes 65936
  191.8 1.3 broadcast_multiply_fusion
  193.1 0.8 fusion.58
  193.9 0.9 multiply_reduce_fusion.2
  195.6 0.8 multiply_convert_fusion.2
  196.3 8.9 %all_gather.11 = bf16[32,128]{1,0:T(8,128)(2,1)S(1)} all-gather(bf16[8,128]{1,0:T(8,128)(2,1)S(1)} %multiply_convert_fusion.2), channel_id=1, replica_groups=mesh['tp'=8,'dp'=4] {'dp'}, dimensions={0}, use_global_device_ids=true | all-gather | bytes 10240 | tf_op jit(solution)/shard_map/all_gather | solution.py:119
  205.2 0.8 fusion.6
  206.7 1.1 pad_maximum_fusion
  208.3 53.2 %all-reduce.20.cloned.1.call-done = f32[32,1024]{1,0:T(8,128)} async-done(((f32[32,1024]{1,0:T(8,128)}), f32[32,1024]{1,0:T(8,128)}) %all-reduce.20.cloned.1.call-update) | async-done | bytes 131088
  261.5 1.4 fusion.37
  (57 shorter events, 8.0 us)
Async XLA Ops:
  7.2 19.1 %copy-start.2 = (bf16[2,1024,128]{2,1,0:T(8,128)(2,1)S(1)}, bf16[2,1024,128]{2,1,0:T(8,128)(2,1)}, u32[]{:S(2)}) copy-start(bf16[2,1024,128]{2,1,0:T(8,128)(2,1)} %param.15) | copy-start | bytes 1572868
  7.2 66.0 %all-reduce.24.cloned.1.call-start = ((), (), s32[]{:S(2)}) async-start(), calls=%async_computation.3 | async-start | bytes 134144
  23.9 3.2 %copy-start.3 = (bf16[2,1024,128]{2,1,0:T(8,128)(2,1)S(1)}, bf16[2,1024,128]{2,1,0:T(8,128)(2,1)}, u32[]{:S(2)}) copy-start(bf16[2,1024,128]{2,1,0:T(8,128)(2,1)} %param.16) | copy-start | bytes 1572868
  23.9 5.7 %copy-start.6 = (bf16[2,1024,16]{1,2,0:T(8,128)(2,1)S(1)}, bf16[2,1024,16]{1,2,0:T(8,128)(2,1)}, u32[]{:S(2)}) copy-start(bf16[2,1024,16]{1,2,0:T(8,128)(2,1)} %param.18) | copy-start | bytes 196612
  23.9 53.8 %copy-start = (f32[2,8,1,128,128]{4,3,2,1,0:T(8,128)S(1)}, f32[2,8,1,128,128]{4,3,2,1,0:T(8,128)}, u32[]{:S(2)}) copy-start(f32[2,8,1,128,128]{4,3,2,1,0:T(8,128)} %param.21) | copy-start | bytes 3145732
  27.8 2.6 copy-start.13
  27.9 3.9 %copy-start.8 = (f32[2,2,1]{1,2,0:T(1,128)S(1)}, f32[2,2,1]{1,2,0:T(1,128)}, u32[]{:S(2)}) copy-start(f32[2,2,1]{1,2,0:T(1,128)} %param.19) | copy-start | bytes 52
  27.9 46.8 %copy-start.9 = (f32[2,8,1]{1,2,0:T(1,128)S(1)}, f32[2,8,1]{1,2,0:T(1,128)}, u32[]{:S(2)}) copy-start(f32[2,8,1]{1,2,0:T(1,128)} %param.23) | copy-start | bytes 196
  27.9 48.2 %copy-start.7 = (f32[2,8,1,128]{3,2,1,0:T(1,128)S(1)}, f32[2,8,1,128]{3,2,1,0:T(1,128)}, u32[]{:S(2)}) copy-start(f32[2,8,1,128]{3,2,1,0:T(1,128)} %param.22) | copy-start | bytes 24580
  29.6 58.1 %copy-start.5 = (bf16[2,128,1024]{2,1,0:T(8,128)(2,1)S(1)}, bf16[2,128,1024]{2,1,0:T(8,128)(2,1)}, u32[]{:S(2)}) copy-start(bf16[2,128,1024]{2,1,0:T(8,128)(2,1)} %param.20) | copy-start | bytes 1572868
  30.4 113.7 %all-reduce.18.cloned.1.call-start = ((), (), s32[]{:S(2)}) async-start(), calls=%async_computation | async-start | bytes 262144 | tf_op jit(solution)/shard_map/psum | solution.py:124
  87.8 57.9 %copy-start.1 = (bf16[2,1024,128]{2,1,0:T(8,128)(2,1)S(1)}, bf16[2,1024,128]{2,1,0:T(8,128)(2,1)}, u32[]{:S(2)}) copy-start(bf16[2,1024,128]{2,1,0:T(8,128)(2,1)} %param.14) | copy-start | bytes 1572868
  88.6 101.7 %all-reduce.22.cloned.1.call-start = ((), (), s32[]{:S(2)}) async-start(), calls=%async_computation.2 | async-start | bytes 134144
  145.7 2.3 copy-start.4
  149.5 112.0 %all-reduce.20.cloned.1.call-start = ((), (), s32[]{:S(2)}) async-start(), calls=%async_computation.1 | async-start | bytes 262144
  149.5 0.7 copy-start.12
  190.4 0.7 copy-start.11
  191.1 0.6 copy-start.10
Sparse Core Ops, SparseCore 0:
  30.5 42.6 all-reduce.23
  88.8 55.2 all-reduce.17
  149.6 40.6 all-reduce.21
  206.2 55.2 all-reduce.19
where the time goes:
time: 270 us; the launch traced here: 269 us
  waiting for transfers between devices  188 us (70%)
  blocking collectives  33.7 us (12%)
  other arithmetic  16.8 us (6%)
  between operations  15.2 us (6%)
  matrix products  11.1 us (4%)
  local copies, waits for them, and re-layouts  3.91 us (1%)
    unnamed x7, waiting for transfers between devices  133 us
    psum x1, waiting for transfers between devices, body(): summed = lax.psum(partial_out, 'tp')  55.4 us
    all_gather x2, blocking collectives, body(): lax.all_gather(gated, 'dp', axis=0, tiled=True)  17.8 us
    all_gather x1, blocking collectives, body(): gathered = lax.all_gather(current, 'tp', axis=0, tiled=True)  15.9 us
  transfers between devices with their start and end apart: 4, of which 4 were waited for; matrix products, arithmetic and copies ran while one was open for 2% of the time, Pallas kernels for 0%

commit v1 on v0

--- a/solution.py
+++ b/solution.py
@@ -121,7 +121,7 @@
             preferred_element_type=jnp.float32,
         )
         if layer_index == 0:
-            summed = lax.psum(partial_out, "tp")
+            summed = lax.all_gather(partial_out, "tp").sum(axis=0)
             gathered = (wide_rows + summed).astype(jnp.bfloat16)
         else:
             current = finish_split(partial_out, wide_rows)

time: 270 us -> 239 us (0.89)
  waiting for transfers between devices: 188 us -> 156 us
    psum x1 -> x0, waiting for transfers between devices: 55.4 us -> none  [body(): summed = lax.psum(partial_out, 'tp')]
    all_gather x0 -> x1, waiting for transfers between devices: none -> 22.7 us  [body(): summed = lax.all_gather(partial_out, 'tp').sum(axis=0)]
where the time goes in v1:
time: 239 us; the launch traced here: 238 us
  waiting for transfers between devices  156 us (65%)
  blocking collectives  33.7 us (14%)
  other arithmetic  17.2 us (7%)
  between operations  15.2 us (6%)
  matrix products  11.2 us (5%)
  local copies, waits for them, and re-layouts  4.3 us (2%)
    unnamed x7, waiting for transfers between devices  134 us
    all_gather x1, waiting for transfers between devices, body(): summed = lax.all_gather(partial_out, 'tp').sum(axis=0)  22.7 us
    all_gather x2, blocking collectives, body(): lax.all_gather(gated, 'dp', axis=0, tiled=True)  17.8 us
    all_gather x1, blocking collectives, body(): gathered = lax.all_gather(current, 'tp', axis=0, tiled=True)  15.9 us
  transfers between devices with their start and end apart: 4, of which 4 were waited for; matrix products, arithmetic and copies ran while one was open for 2% of the time, Pallas kernels for 0%

profile of v1, /device:TPU:0, one launch (start us, length us, event | category | flops | bytes accessed | tf_op | source)
XLA Modules:
  0.0 238.1 jit_solution(6166163460917791186)
XLA Ops:
  7.2 0.8 slice_convert_fusion
  8.0 15.9 %all-gather.1 = bf16[8,4,1024]{2,1,0:T(4,128)(2,1)S(1)} all-gather(bf16[1,4,1024]{2,1,0:T(4,128)(2,1)} %bitcast.148), channel_id=1, replica_groups=mesh['tp'=8,'dp'=4] {'tp'}, dimensions={0}, use_global_device_ids=true | all-gather | bytes 73728 | tf_op jit(solution)/shard_map/all_gather | solution.py:69
  24.6 1.7 fusion.18
  26.3 0.8 fusion.20
  27.1 0.8 fusion.22
  27.9 1.8 fusion.24
  29.7 0.7 fusion.42
  32.4 40.8 %all-reduce.21.cloned.1.call-done = (f32[32,128]{1,0:T(8,128)}, f32[32]{0:T(128)}, f32[32,128]{1,0:T(8,128)}, f32[32,128]{1,0:T(8,128)}, f32[32,2]{0,1:T(2,128)}, /*index=5*/f32[32,128]{1,0:T(8,128)}) async-done(((f32[32,128]{1,0:T(8,128)}, f32[32]{0:T(128)}, f32[32,128]{1,0:T(8,128)}, f32[32,128]{1,0:T(8,128)}, f32[32,2]{0,1:T(2,128)}, /*index=5*/f32[32,128]{1,0:T(8,128)}), (f32[32,128]{1,0:T(8,128)}, ...) | async-done | bytes 65936
  73.2 0.7 add_rsqrt_fusion.1
  74.0 0.7 fusion.62
  74.7 1.4 broadcast_multiply_fusion.1
  76.1 0.8 fusion.59
  76.8 0.9 multiply_reduce_fusion.3
  78.1 0.8 multiply_convert_fusion.3
  78.9 8.9 %all_gather.16 = bf16[32,128]{1,0:T(8,128)(2,1)S(1)} all-gather(bf16[8,128]{1,0:T(8,128)(2,1)S(1)} %multiply_convert_fusion.3), channel_id=1, replica_groups=mesh['tp'=8,'dp'=4] {'dp'}, dimensions={0}, use_global_device_ids=true | all-gather | bytes 10240 | tf_op jit(solution)/shard_map/all_gather | solution.py:119
  87.8 0.8 fusion.16
  88.7 22.7 %all-gather.4.cloned.1.call-done = f32[256,1024]{1,0:T(8,128)} async-done(((f32[32,1024]{1,0:T(8,128)}), f32[256,1024]{1,0:T(8,128)}) %all-gather.4.cloned.1.call-update) | async-done | bytes 1048592 | tf_op jit(solution)/shard_map/all_gather | solution.py:124
  111.4 1.3 reduce_sum.66
  113.7 0.8 fusion.8
  114.5 0.8 fusion.10
  115.3 0.8 fusion.12
  116.1 0.8 fusion.14
  119.5 39.5 %all-reduce.19.cloned.1.call-done = (f32[32,128]{1,0:T(8,128)}, f32[32]{0:T(128)}, f32[32,128]{1,0:T(8,128)}, f32[32,128]{1,0:T(8,128)}, f32[32,2]{0,1:T(2,128)}, /*index=5*/f32[32,128]{1,0:T(8,128)}) async-done(((f32[32,128]{1,0:T(8,128)}, f32[32]{0:T(128)}, f32[32,128]{1,0:T(8,128)}, f32[32,128]{1,0:T(8,128)}, f32[32,2]{0,1:T(2,128)}, /*index=5*/f32[32,128]{1,0:T(8,128)}), (f32[32,128]{1,0:T(8,128)}, ...) | async-done | bytes 65936
  160.4 1.3 broadcast_multiply_fusion
  161.7 0.8 fusion.58
  162.5 0.9 multiply_reduce_fusion.2
  164.2 0.8 multiply_convert_fusion.2
  165.0 8.9 %all_gather.19 = bf16[32,128]{1,0:T(8,128)(2,1)S(1)} all-gather(bf16[8,128]{1,0:T(8,128)(2,1)S(1)} %multiply_convert_fusion.2), channel_id=1, replica_groups=mesh['tp'=8,'dp'=4] {'dp'}, dimensions={0}, use_global_device_ids=true | all-gather | bytes 10240 | tf_op jit(solution)/shard_map/all_gather | solution.py:119
  173.9 0.8 fusion.6
  175.3 1.1 pad_maximum_fusion
  176.9 53.2 %all-reduce.17.cloned.1.call-done = f32[32,1024]{1,0:T(8,128)} async-done(((f32[32,1024]{1,0:T(8,128)}), f32[32,1024]{1,0:T(8,128)}) %all-reduce.17.cloned.1.call-update) | async-done | bytes 131088
  230.2 1.4 fusion.37
  (60 shorter events, 9.1 us)
Async XLA Ops:
  7.2 19.1 %copy-start.2 = (bf16[2,1024,128]{2,1,0:T(8,128)(2,1)S(1)}, bf16[2,1024,128]{2,1,0:T(8,128)(2,1)}, u32[]{:S(2)}) copy-start(bf16[2,1024,128]{2,1,0:T(8,128)(2,1)} %param.15) | copy-start | bytes 1572868
  7.2 66.1 %all-reduce.21.cloned.1.call-start = ((), (), s32[]{:S(2)}) async-start(), calls=%async_computation.3 | async-start | bytes 134144
  23.9 3.2 %copy-start.3 = (bf16[2,1024,128]{2,1,0:T(8,128)(2,1)S(1)}, bf16[2,1024,128]{2,1,0:T(8,128)(2,1)}, u32[]{:S(2)}) copy-start(bf16[2,1024,128]{2,1,0:T(8,128)(2,1)} %param.16) | copy-start | bytes 1572868
  23.9 5.7 %copy-start.7 = (bf16[2,1024,16]{1,2,0:T(8,128)(2,1)S(1)}, bf16[2,1024,16]{1,2,0:T(8,128)(2,1)}, u32[]{:S(2)}) copy-start(bf16[2,1024,16]{1,2,0:T(8,128)(2,1)} %param.18) | copy-start | bytes 196612
  23.9 53.8 %copy-start = (f32[2,8,1,128,128]{4,3,2,1,0:T(8,128)S(1)}, f32[2,8,1,128,128]{4,3,2,1,0:T(8,128)}, u32[]{:S(2)}) copy-start(f32[2,8,1,128,128]{4,3,2,1,0:T(8,128)} %param.21) | copy-start | bytes 3145732
  27.8 2.6 %copy-start.14 = (u32[32]{0:T(128)S(1)}, u32[32]{0:T(128)}, u32[]{:S(2)}) copy-start(u32[32]{0:T(128)} %constant.49) | copy-start | bytes 388
  27.8 3.9 %copy-start.9 = (f32[2,2,1]{1,2,0:T(1,128)S(1)}, f32[2,2,1]{1,2,0:T(1,128)}, u32[]{:S(2)}) copy-start(f32[2,2,1]{1,2,0:T(1,128)} %param.19) | copy-start | bytes 52
  27.8 46.8 %copy-start.10 = (f32[2,8,1]{1,2,0:T(1,128)S(1)}, f32[2,8,1]{1,2,0:T(1,128)}, u32[]{:S(2)}) copy-start(f32[2,8,1]{1,2,0:T(1,128)} %param.23) | copy-start | bytes 196
  27.9 48.2 %copy-start.8 = (f32[2,8,1,128]{3,2,1,0:T(1,128)S(1)}, f32[2,8,1,128]{3,2,1,0:T(1,128)}, u32[]{:S(2)}) copy-start(f32[2,8,1,128]{3,2,1,0:T(1,128)} %param.22) | copy-start | bytes 24580
  29.6 58.1 %copy-start.5 = (bf16[2,128,1024]{2,1,0:T(8,128)(2,1)S(1)}, bf16[2,128,1024]{2,1,0:T(8,128)(2,1)}, u32[]{:S(2)}) copy-start(bf16[2,128,1024]{2,1,0:T(8,128)(2,1)} %param.20) | copy-start | bytes 1572868
  30.4 81.0 %all-gather.4.cloned.1.call-start = ((), (), s32[]{:S(2)}) async-start(), calls=%async_computation | async-start | bytes 1179648 | tf_op jit(solution)/shard_map/all_gather | solution.py:124
  88.6 70.3 %all-reduce.19.cloned.1.call-start = ((), (), s32[]{:S(2)}) async-start(), calls=%async_computation.2 | async-start | bytes 134144
  112.7 1.0 copy-start.1
  113.7 2.3 copy-start.4
  117.6 112.6 %all-reduce.17.cloned.1.call-start = ((), (), s32[]{:S(2)}) async-start(), calls=%async_computation.1 | async-start | bytes 262144
  117.6 0.7 copy-start.13
  159.0 0.7 copy-start.12
  159.7 0.6 copy-start.11
  163.8 10.1 %copy-start.6 = (bf16[2,128,1024]{2,1,0:T(8,128)(2,1)S(1)}, bf16[2,128,1024]{2,1,0:T(8,128)(2,1)}, u32[]{:S(2)}) copy-start(bf16[2,128,1024]{2,1,0:T(8,128)(2,1)} %param.20) | copy-start | bytes 1572868
Sparse Core Ops, SparseCore 0:
  30.5 42.6 all-reduce.20
  88.8 22.6 all-gather.3
  117.7 41.2 all-reduce.18
  174.8 55.3 all-reduce.16
